TPU v7x, 32 devices: a whole 2x2x4 slice. The times are simulated.
32 devices in a mesh: ep: 16 (over z, y, x), tp: 2 (over core).
Axes of the slice: x: 2, y: 2, z: 4, core: 2. Of those that a mesh axis runs over, the one named last changes fastest.
Arguments:
- tokens: bfloat16 [512, 2048], P('ep'), may hold values from -6 to 6
- mix_gain: float32 [2048], replicated, may hold values from 0.1 to 1.9
- w_query: bfloat16 [2048, 512], P('ep', 'tp'), may hold values from -0.125 to 0.125
- w_key: bfloat16 [2048, 512], P('ep', 'tp'), may hold values from -0.125 to 0.125
- w_value: bfloat16 [2048, 512], P('ep', 'tp'), may hold values from -0.125 to 0.125
- w_outgate: bfloat16 [2048, 512], P('ep', 'tp'), may hold values from -0.125 to 0.125
- w_igate: bfloat16 [2048, 8], P('ep', 'tp'), may hold values from -0.125 to 0.125
- w_fgate: bfloat16 [2048, 8], P('ep', 'tp'), may hold values from -0.125 to 0.125
- igate_bias: float32 [8], P('tp'), may hold values from -2 to 1
- fgate_bias: float32 [8], P('tp'), may hold values from 0 to 4
- head_gain: float32 [512], P('tp'), may hold values from 0.1 to 1.9
- w_out: bfloat16 [512, 2048], P('tp', 'ep'), may hold values from -0.25 to 0.25
- state_matrix: float32 [512, 8, 64, 64], P('ep', 'tp'), may hold values from -2.4 to 2.4
- state_norm: float32 [512, 8, 64], P('ep', 'tp'), may hold values from -2.4 to 2.4
- state_max: float32 [512, 8], P('ep', 'tp'), may hold values from -4 to 4
- ffn_gain: float32 [2048], replicated, may hold values from 0.1 to 1.9
- w_expert_gate: bfloat16 [16, 2048, 1408], P('ep', None, 'tp'), may hold values from -0.125 to 0.125
- w_expert_up: bfloat16 [16, 2048, 1408], P('ep', None, 'tp'), may hold values from -0.125 to 0.125
- w_expert_down: bfloat16 [16, 1408, 2048], P('ep', 'tp'), may hold values from -0.15625 to 0.15625
- routes: int32 [512, 3], P('ep'), may hold values from 0 to 15, all different within a row; in each aligned block of 32 rows (0 to 31, 32 to 63, ...) at most 12 rows name the same one
- route_weights: float32 [512, 3], P('ep'), may hold values from 0.2 to 1
Outputs:
- mixed: bfloat16 [512, 2048], P('ep')
- new_matrix: float32 [512, 8, 64, 64], P('ep', 'tp')
- new_norm: float32 [512, 8, 64], P('ep', 'tp')
- new_max: float32 [512, 8], P('ep', 'tp')
Inputs may be any that keep to these rules, and one draw needn't show every extreme that they name: `routes`: each row names 3 different experts. Among the rows of one device, no expert is named by more than 12 rows, a bound that some block reaches.
All inputs are finite; a program needn't handle non-finite values.
Results may differ from a plain program's by a relative error of at most 0.017.
Values may be sent and summed in bfloat16 or wider, within the bound.
No kernel may reach another device: no remote copies, remote signals or barrier semaphores. Data moves between devices by JAX's collectives and lax.ppermute only.
A program may use at most 128 MiB of HBM per device.

v0:
```python
import jax
import jax.numpy as jnp
from jax import lax
from jax.sharding import PartitionSpec as P


def rms_scale(values_in, gain_vec):
    widened = values_in.astype(jnp.float32)
    return (
        widened * lax.rsqrt(jnp.mean(widened * widened, axis=-1, keepdims=True) + 1e-06) * gain_vec
    )


def memory_cell(
    query,
    key_row,
    value_row,
    outgate,
    input_pre,
    forget_pre,
    head_gain,
    state_matrix,
    state_norm,
    state_max,
):
    seq_rows, head_count = input_pre.shape
    head_size = query.shape[1] // head_count
    query_heads = query.astype(jnp.float32).reshape(seq_rows, head_count, head_size)
    key_heads = key_row.astype(jnp.float32).reshape(
        seq_rows, head_count, head_size
    ) * head_size ** (-0.5)
    value_heads = value_row.astype(jnp.float32).reshape(seq_rows, head_count, head_size)
    log_forget = jax.nn.log_sigmoid(forget_pre)
    new_max = jnp.maximum(log_forget + state_max, input_pre)
    keep_old = jnp.exp(log_forget + state_max - new_max)
    keep_new = jnp.exp(input_pre - new_max)
    new_matrix = (
        keep_old[:, :, None, None] * state_matrix
        + keep_new[:, :, None, None] * value_heads[:, :, :, None] * key_heads[:, :, None, :]
    )
    new_norm = keep_old[:, :, None] * state_norm + keep_new[:, :, None] * key_heads
    numerator = jnp.einsum(
        "bhvd,bhd->bhv", new_matrix, query_heads, precision=lax.Precision.HIGHEST
    )
    denominator = jnp.sum(new_norm * query_heads, axis=-1)
    cell_read = numerator / jnp.maximum(jnp.abs(denominator), jnp.exp(-new_max))[:, :, None]
    centered = cell_read - jnp.mean(cell_read, axis=-1, keepdims=True)
    variance = jnp.mean(centered * centered, axis=-1, keepdims=True)
    scaled_cell = (centered * lax.rsqrt(variance + 1e-06)).reshape(seq_rows, head_count * head_size)
    cell_out = (scaled_cell * head_gain * jax.nn.sigmoid(outgate.astype(jnp.float32))).astype(
        jnp.bfloat16
    )
    return (cell_out, new_matrix, new_norm, new_max)


def body(
    tokens,
    mix_gain,
    w_query,
    w_key,
    w_value,
    w_outgate,
    w_igate,
    w_fgate,
    igate_bias,
    fgate_bias,
    head_gain,
    w_out,
    state_matrix,
    state_norm,
    state_max,
    ffn_gain,
    w_expert_gate,
    w_expert_up,
    w_expert_down,
    routes,
    route_weights,
):
    seq_rows, width = tokens.shape
    normed = rms_scale(tokens, mix_gain).astype(jnp.bfloat16)
    weight_list = (w_query, w_key, w_value, w_outgate, w_igate, w_fgate)
    spread = lax.all_to_all(normed, "ep", split_axis=1, concat_axis=0, tiled=True)
    joined = jnp.concatenate(weight_list, axis=1)
    summed = lax.psum_scatter(
        jnp.dot(spread, joined, preferred_element_type=jnp.float32),
        "ep",
        scatter_dimension=0,
        tiled=True,
    )
    bounds = [0]
    for weight in weight_list:
        bounds.append(bounds[-1] + weight.shape[1])
    projected = tuple(
        (summed[:, bounds[index] : bounds[index + 1]] for index in range(len(weight_list)))
    )
    query = projected[0].astype(jnp.bfloat16)
    key_row = projected[1].astype(jnp.bfloat16)
    value_row = projected[2].astype(jnp.bfloat16)
    outgate = projected[3].astype(jnp.bfloat16)
    input_pre = projected[4] + igate_bias
    forget_pre = projected[5] + fgate_bias
    cell_out, new_matrix, new_norm, new_max = memory_cell(
        query,
        key_row,
        value_row,
        outgate,
        input_pre,
        forget_pre,
        head_gain,
        state_matrix,
        state_norm,
        state_max,
    )
    partial_out = jnp.dot(
        cell_out,
        lax.all_gather(w_out, "ep", axis=1, tiled=True),
        preferred_element_type=jnp.float32,
    )
    attended = lax.psum(partial_out.astype(jnp.bfloat16), "tp").astype(jnp.float32)
    resid = (tokens.astype(jnp.float32) + attended).astype(jnp.bfloat16)
    normed_two = rms_scale(resid, ffn_gain).astype(jnp.bfloat16)
    ep_count = lax.axis_size("ep")
    local_experts = w_expert_gate.shape[0]
    expert_total = local_experts * ep_count
    top_count = routes.shape[1]
    capacity = max(2, 2 * seq_rows * top_count // expert_total)
    flat_routes = routes.reshape(-1)
    onehot = (flat_routes[:, None] == jnp.arange(expert_total, dtype=jnp.int32)[None, :]).astype(
        jnp.int32
    )
    earlier = jnp.cumsum(onehot, axis=0, dtype=jnp.int32) - onehot
    slots = jnp.sum(onehot * earlier, axis=1, dtype=jnp.int32)
    targets = flat_routes * capacity + slots
    dispatch = (
        targets[:, None] == jnp.arange(expert_total * capacity, dtype=jnp.int32)[None, :]
    ).astype(jnp.bfloat16)
    route_rows = jnp.repeat(normed_two, top_count, axis=0)
    outgoing = jnp.einsum(
        "rs,rd->sd", dispatch, route_rows, preferred_element_type=jnp.float32
    ).astype(jnp.bfloat16)
    outgoing = outgoing.reshape(expert_total, capacity, width)
    received = lax.all_to_all(outgoing, "ep", split_axis=0, concat_axis=0, tiled=True)
    slot_count = received.shape[1]
    regrouped = received.reshape(ep_count, local_experts, slot_count, width)
    gate_pre = jnp.einsum(
        "nxcd,xdf->nxcf", regrouped, w_expert_gate, preferred_element_type=jnp.float32
    )
    up_pre = jnp.einsum(
        "nxcd,xdf->nxcf", regrouped, w_expert_up, preferred_element_type=jnp.float32
    )
    hidden = (jax.nn.silu(gate_pre) * up_pre).astype(jnp.bfloat16)
    partial_down = jnp.einsum(
        "nxcf,xfd->nxcd", hidden, w_expert_down, preferred_element_type=jnp.float32
    )
    expert_sum = lax.psum(partial_down.astype(jnp.bfloat16), "tp")
    finished = expert_sum.reshape(ep_count * local_experts, slot_count, width)
    returned = lax.all_to_all(finished, "ep", split_axis=0, concat_axis=0, tiled=True)
    picked = jnp.dot(
        dispatch,
        returned.reshape(expert_total * capacity, width),
        preferred_element_type=jnp.float32,
    )
    weighted = jnp.sum(
        picked.reshape(seq_rows, top_count, width) * route_weights[:, :, None], axis=1
    )
    mixed = (resid.astype(jnp.float32) + weighted).astype(jnp.bfloat16)
    return (mixed, new_matrix, new_norm, new_max)


def solution(mesh):
    placed = (
        P("ep", None),
        P(),
        P("ep", "tp"),
        P("ep", "tp"),
        P("ep", "tp"),
        P("ep", "tp"),
        P("ep", "tp"),
        P("ep", "tp"),
        P("tp"),
        P("tp"),
        P("tp"),
        P("tp", "ep"),
        P("ep", "tp", None, None),
        P("ep", "tp", None),
        P("ep", "tp"),
        P(),
        P("ep", None, "tp"),
        P("ep", None, "tp"),
        P("ep", "tp", None),
        P("ep", None),
        P("ep", None),
    )
    return jax.shard_map(
        body,
        mesh=mesh,
        in_specs=placed,
        out_specs=(P("ep", None), P("ep", "tp", None, None), P("ep", "tp", None), P("ep", "tp")),
        check_vma=False,
    )
```

profile of v0, /device:TPU:8, one launch (start us, length us, event | category | flops | bytes accessed | tf_op | source)
XLA Modules:
  0.0 342.0 jit_solution(8380659892496630698)
XLA Ops:
  7.2 1.2 fusion.36
  8.4 1.7 copy_bitcast_fusion
  10.1 7.2 %all-to-all-start = ((bf16[32,16,128]{2,0,1:T(8,128)(2,1)}), bf16[32,16,128]{2,0,1:T(8,128)(2,1)S(1)}, u32[]{:S(2)}, u32[]{:S(2)}) async-start(bf16[32,16,128]{2,0,1:T(8,128)(2,1)} %copy_bitcast_fusion), calls=%async_computation | async-start | bytes 262144 | tf_op jit(solution)/shard_map/all_to_all | solution.py:82
  17.3 0.8 copy.58
  19.0 1.1 concatenate.3
  20.0 3.9 %all-to-all-done = bf16[32,16,128]{2,0,1:T(8,128)(2,1)S(1)} async-done(((bf16[32,16,128]{2,0,1:T(8,128)(2,1)}), bf16[32,16,128]{2,0,1:T(8,128)(2,1)S(1)}, u32[]{:S(2)}, u32[]{:S(2)}) %all-to-all-start) | async-done | bytes 131104 | tf_op jit(solution)/shard_map/all_to_all | solution.py:82
  23.9 1.9 fusion.62
  27.3 125.7 %reduce-scatter.2.cloned.1.call-done = f32[32,1032]{1,0:T(8,128)} async-done(((f32[512,1032]{1,0:T(8,128)}), f32[32,1032]{1,0:T(8,128)}) %reduce-scatter.2.cloned.1.call-update) | async-done | bytes 132112 | tf_op jit(solution)/shard_map/reduce_scatter | solution.py:84
  153.0 0.9 convert.9
  154.4 0.9 broadcast_multiply_fusion.3
  155.3 0.8 subtract_exponential_fusion.1
  156.9 3.8 %multiply_add_fusion = f32[32,4,64,64]{3,2,1,0:T(8,128)S(1)} fusion(f32[32,4,64,64]{3,2,1,0:T(8,128)} %param.33, f32[32,4,64]{2,1,0:T(4,128)S(1)} %get-tuple-element.30, f32[32,4,64]{2,1,0:T(4,128)S(1)} %get-tuple-element.31, f32[32,4]{1,0:T(8,128)S(1)} %subtract_exponential_fusion.1), kind=kLoop, calls=%fused_computation | loop fusion | flops 1572864 | bytes 4260352 | tf_op jit(solution)/shard_map/add | solution.py:38
  160.7 2.0 copy-done.1
  162.7 3.4 fusion.63
  166.7 39.0 %all-gather.2.cloned.1.call-done = bf16[256,2048]{1,0:T(8,128)(2,1)} async-done(((bf16[256,128]{1,0:T(8,128)(2,1)}), bf16[256,2048]{1,0:T(8,128)(2,1)}) %all-gather.2.cloned.1.call-update) | async-done | bytes 1048592 | tf_op jit(solution)/shard_map/all_gather | solution.py:116
  205.7 2.2 convolution_convert_fusion.1
  208.4 18.1 %all-reduce.3.cloned.1.call-done = bf16[32,2048]{1,0:T(8,128)(2,1)} async-done(((bf16[32,2048]{1,0:T(8,128)(2,1)}), bf16[32,2048]{1,0:T(8,128)(2,1)}) %all-reduce.3.cloned.1.call-update) | async-done | bytes 131088 | tf_op jit(solution)/shard_map/psum | solution.py:119
  226.5 1.1 fusion.40
  227.6 1.0 fusion.42
  228.8 1.1 reshape.153
  229.9 2.4 convolution_convert_fusion
  232.3 2.1 reshape.154
  234.4 33.1 %all_to_all.29 = bf16[16,12,2048]{2,1,0:T(8,128)(2,1)S(1)} all-to-all(bf16[16,12,2048]{2,1,0:T(8,128)(2,1)} %reshape.154), channel_id=1, replica_groups=mesh['ep'=16,'tp'=2] {'ep'}, dimensions={0} | all-to-all | bytes 1572864 | tf_op jit(solution)/shard_map/all_to_all | solution.py:142
  267.5 1.0 copy-done.4
  268.5 3.8 %fusion.9 = f32[16,1,12,704]{3,0,2,1:T(8,128)} fusion(bf16[1,2048,704]{1,2,0:T(8,128)(2,1)} %param.37, bf16[16,12,2048]{2,1,0:T(8,128)(2,1)S(1)} %all_to_all.29), kind=kOutput, calls=%fused_computation.11 | convolution fusion | flops 553648128 | bytes 4210688 | tf_op jit(solution)/shard_map/nxcd,xdf->nxcf/dot_general | solution.py:145
  272.3 5.2 %fusion.6 = bf16[16,12,2048]{2,0,1:T(8,128)(2,1)} fusion(bf16[1,704,2048]{2,1,0:T(8,128)(2,1)S(1)} %copy-done, bf16[1,2048,704]{1,2,0:T(8,128)(2,1)} %param.38, f32[16,1,12,704]{3,0,2,1:T(8,128)} %fusion.9, bf16[16,12,2048]{2,1,0:T(8,128)(2,1)} %copy-done.4), kind=kOutput, calls=%fused_computation.7 | convolution fusion | flops 1108500480 | bytes 7880704 | tf_op jit(solution)/shard_map/nxcf,xfd->nxcd/dot_general | solution.py:152
  277.6 17.9 %all-reduce.5.cloned.1.call-done = bf16[16,12,2048]{2,0,1:T(8,128)(2,1)} async-done(((bf16[16,12,2048]{2,0,1:T(8,128)(2,1)}), bf16[16,12,2048]{2,0,1:T(8,128)(2,1)}) %all-reduce.5.cloned.1.call-update) | async-done | bytes 786448 | tf_op jit(solution)/shard_map/psum | solution.py:155
  295.5 2.6 copy.65
  298.1 7.1 %all-to-all-start.2 = ((bf16[16,12,2048]{2,1,0:T(8,128)(2,1)}), bf16[16,12,2048]{2,1,0:T(8,128)(2,1)}, u32[]{:S(2)}, u32[]{:S(2)}) async-start(bf16[16,12,2048]{2,1,0:T(8,128)(2,1)} %copy.65), calls=%async_computation.3 | async-start | bytes 2097152 | tf_op jit(solution)/shard_map/all_to_all | solution.py:157
  306.0 25.1 %all-to-all-done.2 = bf16[16,12,2048]{2,1,0:T(8,128)(2,1)} async-done(((bf16[16,12,2048]{2,1,0:T(8,128)(2,1)}), bf16[16,12,2048]{2,1,0:T(8,128)(2,1)}, u32[]{:S(2)}, u32[]{:S(2)}) %all-to-all-start.2) | async-done | bytes 786464 | tf_op jit(solution)/shard_map/all_to_all | solution.py:157
  331.1 2.1 reshape.169
  333.2 1.5 fusion.18
  (67 shorter events, 6.6 us)
Async XLA Ops:
  7.2 265.2 %copy-start = (bf16[1,704,2048]{2,1,0:T(8,128)(2,1)S(1)}, bf16[1,704,2048]{2,1,0:T(8,128)(2,1)}, u32[]{:S(2)}) copy-start(bf16[1,704,2048]{2,1,0:T(8,128)(2,1)} %param.39) | copy-start | bytes 8650756
  10.1 13.8 %all-to-all-start = ((bf16[32,16,128]{2,0,1:T(8,128)(2,1)}), bf16[32,16,128]{2,0,1:T(8,128)(2,1)S(1)}, u32[]{:S(2)}, u32[]{:S(2)}) async-start(bf16[32,16,128]{2,0,1:T(8,128)(2,1)} %copy_bitcast_fusion), calls=%async_computation | async-start | bytes 262144 | tf_op jit(solution)/shard_map/all_to_all | solution.py:82
  17.3 135.7 %reduce-scatter.2.cloned.1.call-start = ((), (), s32[]{:S(2)}) async-start(), calls=%async_computation.4 | async-start | bytes 2506752 | tf_op jit(solution)/shard_map/reduce_scatter | solution.py:84
  18.9 7.6 %copy-start.13 = (f32[32,4]{0,1:T(4,128)S(1)}, f32[32,4]{0,1:T(4,128)}, u32[]{:S(2)}) copy-start(f32[32,4]{0,1:T(4,128)} %param.35) | copy-start | bytes 1540
  18.9 7.7 %copy-start.7 = (s32[32,3]{0,1:T(4,128)S(1)}, s32[32,3]{0,1:T(4,128)}, u32[]{:S(2)}) copy-start(s32[32,3]{0,1:T(4,128)} %param.40) | copy-start | bytes 1156
  23.9 130.5 %copy-start.10 = (f32[4]{0:T(128)S(1)}, f32[4]{0:T(128)}, u32[]{:S(2)}) copy-start(f32[4]{0:T(128)} %param.30) | copy-start | bytes 52
  23.9 130.5 %copy-start.15 = (f32[4]{0:T(128)S(1)}, f32[4]{0:T(128)}, u32[]{:S(2)}) copy-start(f32[4]{0:T(128)} %param.29) | copy-start | bytes 52
  23.9 132.2 %copy-start.5 = (f32[32,4,64]{2,1,0:T(4,128)S(1)}, f32[32,4,64]{2,1,0:T(4,128)}, u32[]{:S(2)}) copy-start(f32[32,4,64]{2,1,0:T(4,128)} %param.34) | copy-start | bytes 98308
  25.8 179.9 %all-gather.2.cloned.1.call-start = ((), (), s32[]{:S(2)}) async-start(), calls=%async_computation.5 | async-start | bytes 1114112 | tf_op jit(solution)/shard_map/all_gather | solution.py:116
  26.5 200.0 %all-reduce.3.cloned.1.call-start = ((), (), s32[]{:S(2)}) async-start(), calls=%async_computation.6 | async-start | bytes 262144 | tf_op jit(solution)/shard_map/psum | solution.py:119
  27.3 180.6 %copy-start.11 = (s32[96]{0:T(128)}, s32[96]{0:T(128)S(1)}, u32[]{:S(2)}) copy-start(s32[96]{0:T(128)S(1)} %select_reduce_fusion) | copy-start | bytes 1156
  160.7 2.0 copy-start.1
  162.7 43.0 %copy-start.14 = (f32[256]{0:T(256)S(1)}, f32[256]{0:T(256)}, u32[]{:S(2)}) copy-start(f32[256]{0:T(256)} %param.31) | copy-start | bytes 3076
  162.7 63.8 %copy-start.2 = (bf16[32,2048]{1,0:T(8,128)(2,1)S(1)}, bf16[32,2048]{1,0:T(8,128)(2,1)}, u32[]{:S(2)}) copy-start(bf16[32,2048]{1,0:T(8,128)(2,1)} %param.21) | copy-start | bytes 393220
  162.7 64.9 %copy-start.6 = (f32[2048]{0:T(1024)S(1)}, f32[2048]{0:T(1024)}, u32[]{:S(2)}) copy-start(f32[2048]{0:T(1024)} %param.36) | copy-start | bytes 24580
  207.9 87.6 %all-reduce.5.cloned.1.call-start = ((), (), s32[]{:S(2)}) async-start(), calls=%async_computation.7 | async-start | bytes 1572864 | tf_op jit(solution)/shard_map/psum | solution.py:155
  267.5 1.0 copy-start.4
  277.5 27.7 %copy-start.12 = (s32[96]{0:T(128)S(1)}, s32[96]{0:T(128)}, u32[]{:S(2)}) copy-start(s32[96]{0:T(128)} %copy-done.11) | copy-start | bytes 1156
  277.5 27.8 %copy-start.8 = (s32[32,3]{0,1:T(4,128)S(1)}, s32[32,3]{0,1:T(4,128)}, u32[]{:S(2)}) copy-start(s32[32,3]{0,1:T(4,128)} %param.40) | copy-start | bytes 1156
  277.6 55.7 %copy-start.9 = (f32[32,3]{0,1:T(4,128)S(1)}, f32[32,3]{0,1:T(4,128)}, u32[]{:S(2)}) copy-start(f32[32,3]{0,1:T(4,128)} %param.41) | copy-start | bytes 1156
  298.1 36.6 %copy-start.3 = (bf16[32,2048]{1,0:T(8,128)(2,1)S(1)}, bf16[32,2048]{1,0:T(8,128)(2,1)}, u32[]{:S(2)}) copy-start(bf16[32,2048]{1,0:T(8,128)(2,1)} %all-reduce.3.cloned.1.call-done) | copy-start | bytes 393220
  298.1 33.0 %all-to-all-start.2 = ((bf16[16,12,2048]{2,1,0:T(8,128)(2,1)}), bf16[16,12,2048]{2,1,0:T(8,128)(2,1)}, u32[]{:S(2)}, u32[]{:S(2)}) async-start(bf16[16,12,2048]{2,1,0:T(8,128)(2,1)} %copy.65), calls=%async_computation.3 | async-start | bytes 2097152 | tf_op jit(solution)/shard_map/all_to_all | solution.py:157
Sparse Core Ops, SparseCore 0:
  25.9 127.0 reduce-scatter.1
  155.7 49.9 all-gather.1
  208.6 17.9 all-reduce.2
  277.7 17.7 all-reduce.4
where the time goes:
time: 343 us; the launch traced here: 342 us
  waiting for transfers between devices  230 us (67%)
  blocking collectives  33.1 us (10%)
  matrix products  20.2 us (6%)
  local copies, waits for them, and re-layouts  15.4 us (4%)
  starting transfers between devices  14.5 us (4%)
  other arithmetic  14.3 us (4%)
  between operations  14 us (4%)
    reduce_scatter x1, waiting for transfers between devices, body(): lax.psum_scatter(jnp.dot(spread, joined, preferred_element_type=jnp.float...  126 us
    all_gather x1, waiting for transfers between devices, body(): lax.all_gather(w_out, 'ep', axis=1, tiled=True)  39 us
    all_to_all x1, blocking collectives, body(): lax.all_to_all(outgoing, 'ep', split_axis=0, concat_axis=0, tiled=True)  33.1 us
    all_to_all x1, waiting for transfers between devices, body(): lax.all_to_all(finished, 'ep', split_axis=0, concat_axis=0, tiled=True)  25.1 us
    psum x1, waiting for transfers between devices, body(): lax.psum(partial_out.astype(jnp.bfloat16), 'tp').astype(jnp.float32)  18.1 us
    psum x1, waiting for transfers between devices, body(): expert_sum = lax.psum(partial_down.astype(jnp.bfloat16), 'tp')  17.9 us
    all_to_all x1, starting transfers between devices, body(): lax.all_to_all(normed, 'ep', split_axis=1, concat_axis=0, tiled=True)  7.22 us
    all_to_all x1, starting transfers between devices, body(): lax.all_to_all(finished, 'ep', split_axis=0, concat_axis=0, tiled=True)  7.11 us
  transfers between devices with their start and end apart: 6, of which 6 were waited for; matrix products, arithmetic and copies ran while one was open for 5% of the time, Pallas kernels for 0%

commit v1 on v0

--- a/solution.py
+++ b/solution.py
@@ -2,6 +2,22 @@
 import jax.numpy as jnp
 from jax import lax
 from jax.sharding import PartitionSpec as P
+
+
+def ring_gather(x, axis, dim):
+    ways, here, step = (lax.axis_size(axis), lax.axis_index(axis), x.shape[dim])
+    shape = [n * ways if d == dim else n for d, n in enumerate(x.shape)]
+    full = lax.dynamic_update_slice_in_dim(jnp.zeros(shape, x.dtype), x, here * step, axis=dim)
+    going_up = going_down = x
+    for far in range(1, ways // 2 + 1):
+        going_up = lax.ppermute(going_up, axis, [(d, (d + 1) % ways) for d in range(ways)])
+        full = lax.dynamic_update_slice_in_dim(full, going_up, (here - far) % ways * step, axis=dim)
+        if 2 * far < ways:
+            going_down = lax.ppermute(going_down, axis, [(d, (d - 1) % ways) for d in range(ways)])
+            full = lax.dynamic_update_slice_in_dim(
+                full, going_down, (here + far) % ways * step, axis=dim
+            )
+    return full
 
 
 def rms_scale(values_in, gain_vec):
@@ -111,11 +127,7 @@
         state_norm,
         state_max,
     )
-    partial_out = jnp.dot(
-        cell_out,
-        lax.all_gather(w_out, "ep", axis=1, tiled=True),
-        preferred_element_type=jnp.float32,
-    )
+    partial_out = jnp.dot(cell_out, ring_gather(w_out, "ep", 1), preferred_element_type=jnp.float32)
     attended = lax.psum(partial_out.astype(jnp.bfloat16), "tp").astype(jnp.float32)
     resid = (tokens.astype(jnp.float32) + attended).astype(jnp.bfloat16)
     normed_two = rms_scale(resid, ffn_gain).astype(jnp.bfloat16)

time: 343 us -> 304 us (0.89)
  waiting for transfers between devices: 230 us -> 154 us
  starting transfers between devices: 14.5 us -> 41.2 us
  local copies, waits for them, and re-layouts: 15.4 us -> 26.8 us
    reduce_scatter x1, waiting for transfers between devices: 126 us -> 74.9 us  [body(): lax.psum_scatter(jnp.dot(spread, joined, preferred_element_type=jnp.float...]
    all_gather x1 -> x0, waiting for transfers between devices: 39 us -> none  [body(): lax.all_gather(w_out, 'ep', axis=1, tiled=True)]
    ppermute x0 -> x15, starting transfers between devices: none -> 26.7 us  [the longest x7 26.1 us: ring_gather(): lax.ppermute(going_down, axis, [(d, (d - 1) % ways) for d in range(ways)])]
    ppermute x0 -> x15, waiting for transfers between devices: none -> 14.8 us  [the longest x8 11.9 us: ring_gather(): lax.ppermute(going_up, axis, [(d, (d + 1) % ways) for d in range(ways)])]
    dynamic_update_slice x0 -> x16, local copies, waits for them, and re-layouts: none -> 10.2 us  [the longest x8 5.19 us: ring_gather(): lax.dynamic_update_slice_in_dim(full, going_up, (here - far) % ways * ste...]
  transfers between devices with their start and end apart: 6 -> 20, of which waited for: 6 -> 17; matrix products, arithmetic and copies ran while one was open for 5% -> 5% of each run, Pallas kernels for 0% -> 0%
where the time goes in v1:
time: 304 us; the launch traced here: 303 us
  waiting for transfers between devices  154 us (51%)
  starting transfers between devices  41.2 us (14%)
  blocking collectives  33.1 us (11%)
  local copies, waits for them, and re-layouts  26.8 us (9%)
  matrix products  20.3 us (7%)
  other arithmetic  14.3 us (5%)
  between operations  14.1 us (5%)
    reduce_scatter x1, waiting for transfers between devices, body(): lax.psum_scatter(jnp.dot(spread, joined, preferred_element_type=jnp.float...  74.9 us
    all_to_all x1, blocking collectives, body(): lax.all_to_all(outgoing, 'ep', split_axis=0, concat_axis=0, tiled=True)  33.1 us
    ppermute x7, starting transfers between devices, ring_gather(): lax.ppermute(going_down, axis, [(d, (d - 1) % ways) for d in range(ways)])  26.1 us
    all_to_all x1, waiting for transfers between devices, body(): lax.all_to_all(finished, 'ep', split_axis=0, concat_axis=0, tiled=True)  25.1 us
    psum x1, waiting for transfers between devices, body(): expert_sum = lax.psum(partial_down.astype(jnp.bfloat16), 'tp')  17.9 us
    psum x1, waiting for transfers between devices, body(): lax.psum(partial_out.astype(jnp.bfloat16), 'tp').astype(jnp.float32)  17 us
    ppermute x8, waiting for transfers between devices, ring_gather(): lax.ppermute(going_up, axis, [(d, (d + 1) % ways) for d in range(ways)])  11.9 us
    all_to_all x1, starting transfers between devices, body(): lax.all_to_all(normed, 'ep', split_axis=1, concat_axis=0, tiled=True)  7.22 us
  transfers between devices with their start and end apart: 20, of which 17 were waited for; matrix products, arithmetic and copies ran while one was open for 5% of the time, Pallas kernels for 0%

profile of v1, /device:TPU:8, one launch (start us, length us, event | category | flops | bytes accessed | tf_op | source)
XLA Modules:
  0.0 303.3 jit_solution(15579684290840699312)
XLA Ops:
  7.2 1.2 fusion.36
  8.4 1.7 copy_bitcast_fusion
  10.1 7.2 %all-to-all-start = ((bf16[32,16,128]{2,0,1:T(8,128)(2,1)}), bf16[32,16,128]{2,0,1:T(8,128)(2,1)S(1)}, u32[]{:S(2)}, u32[]{:S(2)}) async-start(bf16[32,16,128]{2,0,1:T(8,128)(2,1)} %copy_bitcast_fusion), calls=%async_computation | async-start | bytes 262144 | tf_op jit(solution)/shard_map/all_to_all | solution.py:98
  20.0 3.8 %all-to-all-done = bf16[32,16,128]{2,0,1:T(8,128)(2,1)S(1)} async-done(((bf16[32,16,128]{2,0,1:T(8,128)(2,1)}), bf16[32,16,128]{2,0,1:T(8,128)(2,1)S(1)}, u32[]{:S(2)}, u32[]{:S(2)}) %all-to-all-start) | async-done | bytes 131104 | tf_op jit(solution)/shard_map/all_to_all | solution.py:98
  23.9 1.9 fusion.62
  25.8 1.5 collective-permute-start.1
  28.7 1.1 broadcast_in_dim.4
  30.4 3.3 %collective-permute-start.3 = (bf16[256,128]{1,0:T(8,128)(2,1)S(1)}, bf16[256,128]{1,0:T(8,128)(2,1)S(1)}, u32[]{:S(2)}, u32[]{:S(2)}) collective-permute-start(bf16[256,128]{1,0:T(8,128)(2,1)S(1)} %collective-permute-done.1), channel_id=1, source_target_pairs={{0,30},{2,0},{4,2},{6,4},{8,6},{10,8},{12,10},{14,12},{16,14},{18,... | collective-permute-start | bytes 196616 | tf_op jit(solution)/shard_map/ppermute | solution.py:16
  35.8 4.0 %collective-permute-start.5 = (bf16[256,128]{1,0:T(8,128)(2,1)S(1)}, bf16[256,128]{1,0:T(8,128)(2,1)S(1)}, u32[]{:S(2)}, u32[]{:S(2)}) collective-permute-start(bf16[256,128]{1,0:T(8,128)(2,1)S(1)} %collective-permute-done.3), channel_id=1, source_target_pairs={{0,30},{2,0},{4,2},{6,4},{8,6},{10,8},{12,10},{14,12},{16,14},{18,... | collective-permute-start | bytes 196616 | tf_op jit(solution)/shard_map/ppermute | solution.py:16
  41.8 4.3 %collective-permute-start.7 = (bf16[256,128]{1,0:T(8,128)(2,1)S(1)}, bf16[256,128]{1,0:T(8,128)(2,1)S(1)}, u32[]{:S(2)}, u32[]{:S(2)}) collective-permute-start(bf16[256,128]{1,0:T(8,128)(2,1)S(1)} %collective-permute-done.5), channel_id=1, source_target_pairs={{0,30},{2,0},{4,2},{6,4},{8,6},{10,8},{12,10},{14,12},{16,14},{18,... | collective-permute-start | bytes 196616 | tf_op jit(solution)/shard_map/ppermute | solution.py:16
  48.6 4.4 %collective-permute-start.9 = (bf16[256,128]{1,0:T(8,128)(2,1)S(1)}, bf16[256,128]{1,0:T(8,128)(2,1)S(1)}, u32[]{:S(2)}, u32[]{:S(2)}) collective-permute-start(bf16[256,128]{1,0:T(8,128)(2,1)S(1)} %collective-permute-done.7), channel_id=1, source_target_pairs={{0,30},{2,0},{4,2},{6,4},{8,6},{10,8},{12,10},{14,12},{16,14},{18,... | collective-permute-start | bytes 196616 | tf_op jit(solution)/shard_map/ppermute | solution.py:16
  55.2 4.2 %collective-permute-start.11 = (bf16[256,128]{1,0:T(8,128)(2,1)S(1)}, bf16[256,128]{1,0:T(8,128)(2,1)S(1)}, u32[]{:S(2)}, u32[]{:S(2)}) collective-permute-start(bf16[256,128]{1,0:T(8,128)(2,1)S(1)} %collective-permute-done.9), channel_id=1, source_target_pairs={{0,30},{2,0},{4,2},{6,4},{8,6},{10,8},{12,10},{14,12},{16,14},{18,... | collective-permute-start | bytes 196616 | tf_op jit(solution)/shard_map/ppermute | solution.py:16
  61.5 4.4 %collective-permute-start.13 = (bf16[256,128]{1,0:T(8,128)(2,1)S(1)}, bf16[256,128]{1,0:T(8,128)(2,1)S(1)}, u32[]{:S(2)}, u32[]{:S(2)}) collective-permute-start(bf16[256,128]{1,0:T(8,128)(2,1)S(1)} %collective-permute-done.11), channel_id=1, source_target_pairs={{0,30},{2,0},{4,2},{6,4},{8,6},{10,8},{12,10},{14,12},{16,14},{18,... | collective-permute-start | bytes 196616 | tf_op jit(solution)/shard_map/ppermute | solution.py:16
  67.6 5.1 %collective-permute-done.12 = bf16[256,128]{1,0:T(8,128)(2,1)S(1)} collective-permute-done((bf16[256,128]{1,0:T(8,128)(2,1)S(1)}, bf16[256,128]{1,0:T(8,128)(2,1)S(1)}, u32[]{:S(2)}, u32[]{:S(2)}) %collective-permute-start.12) | collective-permute-done | bytes 65568 | tf_op jit(solution)/shard_map/ppermute | solution.py:13
  74.1 4.8 %collective-permute-done.14 = bf16[256,128]{1,0:T(8,128)(2,1)S(1)} collective-permute-done((bf16[256,128]{1,0:T(8,128)(2,1)S(1)}, bf16[256,128]{1,0:T(8,128)(2,1)S(1)}, u32[]{:S(2)}, u32[]{:S(2)}) %collective-permute-start.14) | collective-permute-done | bytes 65568 | tf_op jit(solution)/shard_map/ppermute | solution.py:13
  79.5 74.9 %reduce-scatter.2.cloned.1.call-done = f32[32,1032]{1,0:T(8,128)} async-done(((f32[512,1032]{1,0:T(8,128)}), f32[32,1032]{1,0:T(8,128)}) %reduce-scatter.2.cloned.1.call-update) | async-done | bytes 132112 | tf_op jit(solution)/shard_map/reduce_scatter | solution.py:100
  158.2 3.8 %multiply_add_fusion = f32[32,4,64,64]{3,2,1,0:T(8,128)S(1)} fusion(f32[32,4,64,64]{3,2,1,0:T(8,128)} %param.33, f32[32,4,64]{2,1,0:T(4,128)S(1)} %get-tuple-element.30, f32[32,4,64]{2,1,0:T(4,128)S(1)} %get-tuple-element.31, f32[32,4]{1,0:T(8,128)S(1)} %subtract_exponential_fusion.1), kind=kLoop, calls=%fused_computation | loop fusion | flops 1572864 | bytes 4260352 | tf_op jit(solution)/shard_map/add | solution.py:54
  162.0 2.0 copy-done.1
  164.0 3.4 %fusion.63 = f32[32,4,1,64]{3,2,1,0:T(1,128)S(1)} fusion(f32[32,4,64,64]{3,2,1,0:T(8,128)S(1)} %multiply_add_fusion, bf16[32,4,64,1]{2,3,1,0:T(2,128)(2,1)S(1)} %reshape.171), kind=kOutput, calls=%fused_computation.100 | convolution fusion | flops 6291456 | bytes 2146304 | tf_op jit(solution)/shard_map/bhvd,bhd->bhv/dot_general | solution.py:58
  168.0 2.2 convolution_convert_fusion.1
  170.8 17.0 %all-reduce.3.cloned.1.call-done = bf16[32,2048]{1,0:T(8,128)(2,1)} async-done(((bf16[32,2048]{1,0:T(8,128)(2,1)}), bf16[32,2048]{1,0:T(8,128)(2,1)}) %all-reduce.3.cloned.1.call-update) | async-done | bytes 131088 | tf_op jit(solution)/shard_map/psum | solution.py:131
  191.2 2.4 convolution_convert_fusion
  193.6 2.1 reshape.154
  195.8 33.1 %all_to_all.29 = bf16[16,12,2048]{2,1,0:T(8,128)(2,1)S(1)} all-to-all(bf16[16,12,2048]{2,1,0:T(8,128)(2,1)} %reshape.154), channel_id=1, replica_groups=mesh['ep'=16,'tp'=2] {'ep'}, dimensions={0} | all-to-all | bytes 1572864 | tf_op jit(solution)/shard_map/all_to_all | solution.py:154
  229.8 3.8 %fusion.9 = f32[16,1,12,704]{3,0,2,1:T(8,128)} fusion(bf16[1,2048,704]{1,2,0:T(8,128)(2,1)} %param.37, bf16[16,12,2048]{2,1,0:T(8,128)(2,1)S(1)} %all_to_all.29), kind=kOutput, calls=%fused_computation.11 | convolution fusion | flops 553648128 | bytes 4210688 | tf_op jit(solution)/shard_map/nxcd,xdf->nxcf/dot_general | solution.py:157
  233.7 5.2 %fusion.6 = bf16[16,12,2048]{2,0,1:T(8,128)(2,1)} fusion(bf16[1,704,2048]{2,1,0:T(8,128)(2,1)S(1)} %copy-done, bf16[1,2048,704]{1,2,0:T(8,128)(2,1)} %param.38, f32[16,1,12,704]{3,0,2,1:T(8,128)} %fusion.9, bf16[16,12,2048]{2,1,0:T(8,128)(2,1)} %copy-done.4), kind=kOutput, calls=%fused_computation.7 | convolution fusion | flops 1108500480 | bytes 7880704 | tf_op jit(solution)/shard_map/nxcf,xfd->nxcd/dot_general | solution.py:164
  238.9 17.9 %all-reduce.5.cloned.1.call-done = bf16[16,12,2048]{2,0,1:T(8,128)(2,1)} async-done(((bf16[16,12,2048]{2,0,1:T(8,128)(2,1)}), bf16[16,12,2048]{2,0,1:T(8,128)(2,1)}) %all-reduce.5.cloned.1.call-update) | async-done | bytes 786448 | tf_op jit(solution)/shard_map/psum | solution.py:167
  256.8 2.6 copy.65
  259.4 7.1 %all-to-all-start.2 = ((bf16[16,12,2048]{2,1,0:T(8,128)(2,1)}), bf16[16,12,2048]{2,1,0:T(8,128)(2,1)}, u32[]{:S(2)}, u32[]{:S(2)}) async-start(bf16[16,12,2048]{2,1,0:T(8,128)(2,1)} %copy.65), calls=%async_computation.3 | async-start | bytes 2097152 | tf_op jit(solution)/shard_map/all_to_all | solution.py:169
  267.4 25.1 %all-to-all-done.2 = bf16[16,12,2048]{2,1,0:T(8,128)(2,1)} async-done(((bf16[16,12,2048]{2,1,0:T(8,128)(2,1)}), bf16[16,12,2048]{2,1,0:T(8,128)(2,1)}, u32[]{:S(2)}, u32[]{:S(2)}) %all-to-all-start.2) | async-done | bytes 786464 | tf_op jit(solution)/shard_map/all_to_all | solution.py:169
  292.4 2.1 reshape.169
  294.6 1.5 fusion.18
  (113 shorter events, 30.2 us)
Async XLA Ops:
  7.2 226.5 %copy-start = (bf16[1,704,2048]{2,1,0:T(8,128)(2,1)S(1)}, bf16[1,704,2048]{2,1,0:T(8,128)(2,1)}, u32[]{:S(2)}) copy-start(bf16[1,704,2048]{2,1,0:T(8,128)(2,1)} %param.39) | copy-start | bytes 8650756
  10.1 13.8 %all-to-all-start = ((bf16[32,16,128]{2,0,1:T(8,128)(2,1)}), bf16[32,16,128]{2,0,1:T(8,128)(2,1)S(1)}, u32[]{:S(2)}, u32[]{:S(2)}) async-start(bf16[32,16,128]{2,0,1:T(8,128)(2,1)} %copy_bitcast_fusion), calls=%async_computation | async-start | bytes 262144 | tf_op jit(solution)/shard_map/all_to_all | solution.py:98
  17.3 137.1 %reduce-scatter.2.cloned.1.call-start = ((), (), s32[]{:S(2)}) async-start(), calls=%async_computation.4 | async-start | bytes 2506752 | tf_op jit(solution)/shard_map/reduce_scatter | solution.py:100
  20.0 8.0 %copy-start.8 = (s32[32,3]{0,1:T(4,128)S(1)}, s32[32,3]{0,1:T(4,128)}, u32[]{:S(2)}) copy-start(s32[32,3]{0,1:T(4,128)} %param.40) | copy-start | bytes 1156
  25.7 129.9 %copy-start.11 = (f32[4]{0:T(128)S(1)}, f32[4]{0:T(128)}, u32[]{:S(2)}) copy-start(f32[4]{0:T(128)} %param.30) | copy-start | bytes 52
  25.7 129.9 %copy-start.16 = (f32[4]{0:T(128)S(1)}, f32[4]{0:T(128)}, u32[]{:S(2)}) copy-start(f32[4]{0:T(128)} %param.29) | copy-start | bytes 52
  25.8 131.6 %copy-start.5 = (f32[32,4,64]{2,1,0:T(4,128)S(1)}, f32[32,4,64]{2,1,0:T(4,128)}, u32[]{:S(2)}) copy-start(f32[32,4,64]{2,1,0:T(4,128)} %param.34) | copy-start | bytes 98308
  25.8 162.0 %all-reduce.3.cloned.1.call-start = ((), (), s32[]{:S(2)}) async-start(), calls=%async_computation.5 | async-start | bytes 262144 | tf_op jit(solution)/shard_map/psum | solution.py:131
  25.8 4.6 %collective-permute-start.1 = (bf16[256,128]{1,0:T(8,128)(2,1)S(1)}, bf16[256,128]{1,0:T(8,128)(2,1)S(1)}, u32[]{:S(2)}, u32[]{:S(2)}) collective-permute-start(bf16[256,128]{1,0:T(8,128)(2,1)S(1)} %copy-done.6), channel_id=1, source_target_pairs={{0,30},{2,0},{4,2},{6,4},{8,6},{10,8},{12,10},{14,12},{16,14},{18,... | collective-permute-start | bytes 196616 | tf_op jit(solution)/shard_map/ppermute | solution.py:16
  27.4 6.3 %collective-permute-start = (bf16[256,128]{1,0:T(8,128)(2,1)S(1)}, bf16[256,128]{1,0:T(8,128)(2,1)S(1)}, u32[]{:S(2)}, u32[]{:S(2)}) collective-permute-start(bf16[256,128]{1,0:T(8,128)(2,1)S(1)} %copy-done.6), channel_id=1, source_target_pairs={{0,2},{2,4},{4,6},{6,8},{8,10},{10,12},{12,14},{14,16},{16,18},{18... | collective-permute-start | bytes 196616 | tf_op jit(solution)/shard_map/ppermute | solution.py:13
  28.7 141.6 %copy-start.12 = (s32[96]{0:T(128)}, s32[96]{0:T(128)S(1)}, u32[]{:S(2)}) copy-start(s32[96]{0:T(128)S(1)} %select_reduce_fusion) | copy-start | bytes 1156
  30.4 5.3 %collective-permute-start.3 = (bf16[256,128]{1,0:T(8,128)(2,1)S(1)}, bf16[256,128]{1,0:T(8,128)(2,1)S(1)}, u32[]{:S(2)}, u32[]{:S(2)}) collective-permute-start(bf16[256,128]{1,0:T(8,128)(2,1)S(1)} %collective-permute-done.1), channel_id=1, source_target_pairs={{0,30},{2,0},{4,2},{6,4},{8,6},{10,8},{12,10},{14,12},{16,14},{18,... | collective-permute-start | bytes 196616 | tf_op jit(solution)/shard_map/ppermute | solution.py:16
  33.7 6.2 %collective-permute-start.2 = (bf16[256,128]{1,0:T(8,128)(2,1)S(1)}, bf16[256,128]{1,0:T(8,128)(2,1)S(1)}, u32[]{:S(2)}, u32[]{:S(2)}) collective-permute-start(bf16[256,128]{1,0:T(8,128)(2,1)S(1)} %collective-permute-done), channel_id=1, source_target_pairs={{0,2},{2,4},{4,6},{6,8},{8,10},{10,12},{12,14},{14,16},{16,18},{18... | collective-permute-start | bytes 196616 | tf_op jit(solution)/shard_map/ppermute | solution.py:13
  35.8 6.0 %collective-permute-start.5 = (bf16[256,128]{1,0:T(8,128)(2,1)S(1)}, bf16[256,128]{1,0:T(8,128)(2,1)S(1)}, u32[]{:S(2)}, u32[]{:S(2)}) collective-permute-start(bf16[256,128]{1,0:T(8,128)(2,1)S(1)} %collective-permute-done.3), channel_id=1, source_target_pairs={{0,30},{2,0},{4,2},{6,4},{8,6},{10,8},{12,10},{14,12},{16,14},{18,... | collective-permute-start | bytes 196616 | tf_op jit(solution)/shard_map/ppermute | solution.py:16
  39.9 6.6 %collective-permute-start.4 = (bf16[256,128]{1,0:T(8,128)(2,1)S(1)}, bf16[256,128]{1,0:T(8,128)(2,1)S(1)}, u32[]{:S(2)}, u32[]{:S(2)}) collective-permute-start(bf16[256,128]{1,0:T(8,128)(2,1)S(1)} %collective-permute-done.2), channel_id=1, source_target_pairs={{0,2},{2,4},{4,6},{6,8},{8,10},{10,12},{12,14},{14,16},{16,18},{18... | collective-permute-start | bytes 196616 | tf_op jit(solution)/shard_map/ppermute | solution.py:13
  41.8 6.8 %collective-permute-start.7 = (bf16[256,128]{1,0:T(8,128)(2,1)S(1)}, bf16[256,128]{1,0:T(8,128)(2,1)S(1)}, u32[]{:S(2)}, u32[]{:S(2)}) collective-permute-start(bf16[256,128]{1,0:T(8,128)(2,1)S(1)} %collective-permute-done.5), channel_id=1, source_target_pairs={{0,30},{2,0},{4,2},{6,4},{8,6},{10,8},{12,10},{14,12},{16,14},{18,... | collective-permute-start | bytes 196616 | tf_op jit(solution)/shard_map/ppermute | solution.py:16
  46.5 7.0 %collective-permute-start.6 = (bf16[256,128]{1,0:T(8,128)(2,1)S(1)}, bf16[256,128]{1,0:T(8,128)(2,1)S(1)}, u32[]{:S(2)}, u32[]{:S(2)}) collective-permute-start(bf16[256,128]{1,0:T(8,128)(2,1)S(1)} %collective-permute-done.4), channel_id=1, source_target_pairs={{0,2},{2,4},{4,6},{6,8},{8,10},{10,12},{12,14},{14,16},{16,18},{18... | collective-permute-start | bytes 196616 | tf_op jit(solution)/shard_map/ppermute | solution.py:13
  48.6 6.6 %collective-permute-start.9 = (bf16[256,128]{1,0:T(8,128)(2,1)S(1)}, bf16[256,128]{1,0:T(8,128)(2,1)S(1)}, u32[]{:S(2)}, u32[]{:S(2)}) collective-permute-start(bf16[256,128]{1,0:T(8,128)(2,1)S(1)} %collective-permute-done.7), channel_id=1, source_target_pairs={{0,30},{2,0},{4,2},{6,4},{8,6},{10,8},{12,10},{14,12},{16,14},{18,... | collective-permute-start | bytes 196616 | tf_op jit(solution)/shard_map/ppermute | solution.py:16
  53.5 6.4 %collective-permute-start.8 = (bf16[256,128]{1,0:T(8,128)(2,1)S(1)}, bf16[256,128]{1,0:T(8,128)(2,1)S(1)}, u32[]{:S(2)}, u32[]{:S(2)}) collective-permute-start(bf16[256,128]{1,0:T(8,128)(2,1)S(1)} %collective-permute-done.6), channel_id=1, source_target_pairs={{0,2},{2,4},{4,6},{6,8},{8,10},{10,12},{12,14},{14,16},{16,18},{18... | collective-permute-start | bytes 196616 | tf_op jit(solution)/shard_map/ppermute | solution.py:13
  55.2 6.3 %collective-permute-start.11 = (bf16[256,128]{1,0:T(8,128)(2,1)S(1)}, bf16[256,128]{1,0:T(8,128)(2,1)S(1)}, u32[]{:S(2)}, u32[]{:S(2)}) collective-permute-start(bf16[256,128]{1,0:T(8,128)(2,1)S(1)} %collective-permute-done.9), channel_id=1, source_target_pairs={{0,30},{2,0},{4,2},{6,4},{8,6},{10,8},{12,10},{14,12},{16,14},{18,... | collective-permute-start | bytes 196616 | tf_op jit(solution)/shard_map/ppermute | solution.py:16
  59.9 6.5 %collective-permute-start.10 = (bf16[256,128]{1,0:T(8,128)(2,1)S(1)}, bf16[256,128]{1,0:T(8,128)(2,1)S(1)}, u32[]{:S(2)}, u32[]{:S(2)}) collective-permute-start(bf16[256,128]{1,0:T(8,128)(2,1)S(1)} %collective-permute-done.8), channel_id=1, source_target_pairs={{0,2},{2,4},{4,6},{6,8},{8,10},{10,12},{12,14},{14,16},{16,18},{18... | collective-permute-start | bytes 196616 | tf_op jit(solution)/shard_map/ppermute | solution.py:13
  61.5 11.9 %collective-permute-start.13 = (bf16[256,128]{1,0:T(8,128)(2,1)S(1)}, bf16[256,128]{1,0:T(8,128)(2,1)S(1)}, u32[]{:S(2)}, u32[]{:S(2)}) collective-permute-start(bf16[256,128]{1,0:T(8,128)(2,1)S(1)} %collective-permute-done.11), channel_id=1, source_target_pairs={{0,30},{2,0},{4,2},{6,4},{8,6},{10,8},{12,10},{14,12},{16,14},{18,... | collective-permute-start | bytes 196616 | tf_op jit(solution)/shard_map/ppermute | solution.py:16
  66.4 6.4 %collective-permute-start.12 = (bf16[256,128]{1,0:T(8,128)(2,1)S(1)}, bf16[256,128]{1,0:T(8,128)(2,1)S(1)}, u32[]{:S(2)}, u32[]{:S(2)}) collective-permute-start(bf16[256,128]{1,0:T(8,128)(2,1)S(1)} %collective-permute-done.10), channel_id=1, source_target_pairs={{0,2},{2,4},{4,6},{6,8},{8,10},{10,12},{12,14},{14,16},{16,18},{18... | collective-permute-start | bytes 196616 | tf_op jit(solution)/shard_map/ppermute | solution.py:13
  72.8 6.1 %collective-permute-start.14 = (bf16[256,128]{1,0:T(8,128)(2,1)S(1)}, bf16[256,128]{1,0:T(8,128)(2,1)S(1)}, u32[]{:S(2)}, u32[]{:S(2)}) collective-permute-start(bf16[256,128]{1,0:T(8,128)(2,1)S(1)} %collective-permute-done.12), channel_id=1, source_target_pairs={{0,2},{2,4},{4,6},{6,8},{8,10},{10,12},{12,14},{14,16},{16,18},{18... | collective-permute-start | bytes 196616 | tf_op jit(solution)/shard_map/ppermute | solution.py:13
  164.0 23.8 %copy-start.2 = (bf16[32,2048]{1,0:T(8,128)(2,1)S(1)}, bf16[32,2048]{1,0:T(8,128)(2,1)}, u32[]{:S(2)}) copy-start(bf16[32,2048]{1,0:T(8,128)(2,1)} %param.21) | copy-start | bytes 393220
  164.0 24.9 %copy-start.7 = (f32[2048]{0:T(1024)S(1)}, f32[2048]{0:T(1024)}, u32[]{:S(2)}) copy-start(f32[2048]{0:T(1024)} %param.36) | copy-start | bytes 24580
  170.2 86.6 %all-reduce.5.cloned.1.call-start = ((), (), s32[]{:S(2)}) async-start(), calls=%async_computation.6 | async-start | bytes 1572864 | tf_op jit(solution)/shard_map/psum | solution.py:167
  238.9 27.6 %copy-start.13 = (s32[96]{0:T(128)S(1)}, s32[96]{0:T(128)}, u32[]{:S(2)}) copy-start(s32[96]{0:T(128)} %copy-done.12) | copy-start | bytes 1156
  238.9 27.8 %copy-start.9 = (s32[32,3]{0,1:T(4,128)S(1)}, s32[32,3]{0,1:T(4,128)}, u32[]{:S(2)}) copy-start(s32[32,3]{0,1:T(4,128)} %param.40) | copy-start | bytes 1156
  238.9 55.7 %copy-start.10 = (f32[32,3]{0,1:T(4,128)S(1)}, f32[32,3]{0,1:T(4,128)}, u32[]{:S(2)}) copy-start(f32[32,3]{0,1:T(4,128)} %param.41) | copy-start | bytes 1156
  259.4 36.7 %copy-start.3 = (bf16[32,2048]{1,0:T(8,128)(2,1)S(1)}, bf16[32,2048]{1,0:T(8,128)(2,1)}, u32[]{:S(2)}) copy-start(bf16[32,2048]{1,0:T(8,128)(2,1)} %all-reduce.3.cloned.1.call-done) | copy-start | bytes 393220
  259.4 33.0 %all-to-all-start.2 = ((bf16[16,12,2048]{2,1,0:T(8,128)(2,1)}), bf16[16,12,2048]{2,1,0:T(8,128)(2,1)}, u32[]{:S(2)}, u32[]{:S(2)}) async-start(bf16[16,12,2048]{2,1,0:T(8,128)(2,1)} %copy.65), calls=%async_computation.3 | async-start | bytes 2097152 | tf_op jit(solution)/shard_map/all_to_all | solution.py:169
  (5 other events, 21.8 us)
Sparse Core Ops, SparseCore 0:
  25.9 128.3 reduce-scatter.1
  170.3 17.4 all-reduce.2
  239.0 17.7 all-reduce.4
